TPU v7x, 32 devices: a whole 2x2x4 slice. The times are simulated.
32 devices in a mesh: ep: 8 (over z, core), tp: 4 (over y, x).
Axes of the slice: x: 2, y: 2, z: 4, core: 2. Of those that a mesh axis runs over, the one named last changes fastest.
Arguments:
- receptance: bfloat16 [2048, 2048], P('ep', 'tp'), may hold values from -6 to 6
- key_tensor: bfloat16 [2048, 2048], P('ep', 'tp'), may hold values from -6 to 6
- value_tensor: bfloat16 [2048, 2048], P('ep', 'tp'), may hold values from -6 to 6
- decay_data_input: bfloat16 [2048, 2048], P('ep', 'tp'), may hold values from -4 to 4
- correction_rate_input: bfloat16 [2048, 2048], P('ep', 'tp'), may hold values from -16 to 6
- mixer_output_gate: bfloat16 [2048, 2048], P('ep', 'tp'), may hold values from -6 to 6
- decay_channel_offset: float32 [2048], P('tp'), may hold values from -16 to -3
- head_norm_gain: float32 [2048], P('tp'), may hold values from 0.1 to 1.9
- self_key_weight: float32 [2048], P('tp'), may hold values from -2 to 2
- mixer_output_weight: bfloat16 [2048, 2048], P('tp'), may hold values from -0.125 to 0.125
- second_batch_rows: bfloat16 [1024, 2048], P('ep'), may hold values from -6 to 6
- routed_expert_index: int32 [1024, 4], P('ep'), may hold values from 0 to 7, all different within a row; in each aligned block of 128 rows (0 to 127, 128 to 255, ...) at most 96 rows name the same one
- routing_output_weight: float32 [1024, 4], P('ep'), may hold values from 0.1 to 1
- expert_norm_gain: float32 [2048], replicated, may hold values from 0.1 to 1.9
- expert_gate_weight: bfloat16 [8, 1024, 2048], P('ep', 'tp'), may hold values from -0.125 to 0.125
- expert_up_weight: bfloat16 [8, 1024, 2048], P('ep', 'tp'), may hold values from -0.125 to 0.125
- expert_down_weight: bfloat16 [8, 1024, 2048], P('ep', None, 'tp'), may hold values from -0.1875 to 0.1875
- common_expert_gate: bfloat16 [1024, 2048], P('tp'), may hold values from -0.125 to 0.125
- common_expert_up: bfloat16 [1024, 2048], P('tp'), may hold values from -0.125 to 0.125
- common_expert_down: bfloat16 [1024, 2048], P(None, 'tp'), may hold values from -0.1875 to 0.1875
Outputs:
- token_mixer_output: bfloat16 [2048, 2048], P(('ep', 'tp'))
- expert_out: bfloat16 [1024, 2048], P('ep', 'tp')
Inputs may be any that keep to these rules, and one draw needn't show every extreme that they name: `routed_expert_index`: each row names 4 different experts. Within the rows of one index of ep no expert is named by more than 96 rows, and that bound is met in some index's rows.
All inputs are finite; a program needn't handle non-finite values.
Results may differ from a plain program's by a relative error of at most 0.017.
Values may be sent and summed in bfloat16 or wider, within the bound.
A program may use at most 128 MiB of HBM per device.

v0:
```python
import math
import jax
import jax.numpy as jnp
from jax import lax
from jax.sharding import PartitionSpec as P

HEAD_CHANNELS = 64
SPAN = 64
HIGHEST = lax.Precision.HIGHEST
PRECISION = lax.Precision.HIGH
NORM_FLOOR = 1.0


def head_view(matrix):
    return matrix.astype(jnp.float32).reshape(matrix.shape[0], -1, HEAD_CHANNELS)


def complete_head_outputs(
    state_readout,
    receptance_rows,
    key_row_block,
    value_row_block,
    head_norm_gain,
    self_key_weight,
    mixer_output_gate,
):
    mean_part = jnp.mean(state_readout, axis=-1, keepdims=True)
    spread = jnp.mean(jnp.square(state_readout - mean_part), axis=-1, keepdims=True)
    normalized_rows = (state_readout - mean_part) * lax.rsqrt(spread + NORM_FLOOR)
    sequence_length = state_readout.shape[0]
    normalized_rows = normalized_rows.reshape(sequence_length, -1) * head_norm_gain
    self_key_term = (
        jnp.sum(
            receptance_rows * key_row_block * self_key_weight.reshape(-1, HEAD_CHANNELS),
            axis=-1,
            keepdims=True,
        )
        * value_row_block
    )
    mixer_result = (
        normalized_rows + self_key_term.reshape(sequence_length, -1)
    ) * mixer_output_gate.astype(jnp.float32)
    return mixer_result.astype(jnp.bfloat16)


def product(spec, left, right):
    return jnp.einsum(spec, left, right, precision=PRECISION, preferred_element_type=jnp.float32)


def lower_inverse(strict, size):
    at = jnp.arange(size)
    row, column = (at[:, None], at[None, :])
    inverse = None
    block = 1
    while block < size:
        pair = (
            (row // (2 * block) == column // (2 * block))
            & (row // block % 2 == 1)
            & (column // block % 2 == 0)
        )
        below = jnp.where(pair, strict, 0.0)
        if inverse is None:
            inverse = jnp.eye(size, dtype=jnp.float32) - below
        else:
            inverse = inverse - product(
                "nhij,nhjk->nhik", product("nhij,nhjk->nhik", inverse, below), inverse
            )
        block *= 2
    return inverse


def mixer_part(
    receptance,
    key_tensor,
    value_tensor,
    decay_data_input,
    correction_rate_input,
    mixer_output_gate,
    decay_channel_offset,
    head_norm_gain,
    self_key_weight,
    mixer_output_weight,
):
    row_count, width = receptance.shape
    head_count = width // HEAD_CHANNELS
    span = min(SPAN, row_count)
    block_count = row_count // span
    receptance_rows = head_view(receptance)
    key_row_block = head_view(key_tensor)
    value_row_block = head_view(value_tensor)

    def by_block(matrix):
        return (
            matrix.astype(jnp.float32)
            .reshape(block_count, span, head_count, HEAD_CHANNELS)
            .transpose(0, 2, 1, 3)
        )

    step_log = -math.exp(-0.5) * jax.nn.sigmoid(
        decay_channel_offset + decay_data_input.astype(jnp.float32)
    )
    at = jnp.arange(span)
    reach = (at[:, None] >= at[None, :]).astype(jnp.float32)
    step_log = by_block(step_log)
    total_log = jnp.einsum("ts,nhsd->nhtd", reach, step_log, precision=HIGHEST)
    recept, keys, values = (by_block(receptance), by_block(key_tensor), by_block(value_tensor))
    units = keys * lax.rsqrt(jnp.sum(keys * keys, axis=-1, keepdims=True) + 1.0)
    corrections = units * jax.nn.sigmoid(by_block(correction_rate_input))
    grown = jnp.exp(-total_log)
    last_log = total_log[:, :, -1:, :]
    unit_in = units * jnp.exp(total_log - step_log)
    recept_in = recept * jnp.exp(total_log)
    tail = jnp.exp(last_log - total_log)
    scores = product(
        "nhtd,nhsd->nhts",
        jnp.concatenate([unit_in, recept_in], axis=2),
        jnp.concatenate([keys * grown, corrections * grown], axis=2),
    )
    before = at[:, None] > at[None, :]
    upto = at[:, None] >= at[None, :]
    unit_key = jnp.where(before, scores[:, :, :span, :span], 0.0)
    unit_fix = jnp.where(before, scores[:, :, :span, span:], 0.0)
    read_key = jnp.where(upto, scores[:, :, span:, :span], 0.0)
    read_fix = jnp.where(upto, scores[:, :, span:, span:], 0.0)
    inverse = lower_inverse(unit_fix, span)
    key_values = product("nhts,nhsd->nhtd", jnp.concatenate([unit_key, read_key], axis=2), values)
    solved = product(
        "nhts,nhsd->nhtd", inverse, jnp.concatenate([unit_in, key_values[:, :, :span]], axis=3)
    )
    reads = jnp.concatenate([recept_in, key_values[:, :, span:]], axis=3) - product(
        "nhts,nhsd->nhtd", read_fix, solved
    )
    eye_head = jnp.eye(HEAD_CHANNELS, dtype=jnp.float32)
    fresh = product("nhtj,nhti->nhji", keys * tail, values)
    moves = jnp.concatenate([eye_head * jnp.exp(last_log), fresh], axis=3) - product(
        "nhtj,nhti->nhji", corrections * tail, solved
    )
    whole = moves[0]
    for block in range(1, block_count):
        step = product("hij,hjk->hik", moves[block, :, :, :HEAD_CHANNELS], whole)
        whole = step + jnp.concatenate(
            [jnp.zeros_like(step[..., :HEAD_CHANNELS]), moves[block, :, :, HEAD_CHANNELS:]], axis=2
        )
    everything = lax.all_gather(whole.astype(jnp.bfloat16), "ep")
    mine = lax.axis_index("ep")
    state = jnp.zeros((head_count, HEAD_CHANNELS, HEAD_CHANNELS), jnp.float32)
    for k in range(lax.axis_size("ep") - 1):
        part = everything[k].astype(jnp.float32)
        new = product("hij,hjk->hik", part[..., :HEAD_CHANNELS], state)
        state = jnp.where(k < mine, new + part[..., HEAD_CHANNELS:], state)
    starts = [state]
    for block in range(block_count - 1):
        state = (
            product("hij,hjk->hik", moves[block, :, :, :HEAD_CHANNELS], state)
            + moves[block, :, :, HEAD_CHANNELS:]
        )
        starts.append(state)
    merged_output = reads[..., HEAD_CHANNELS:] + product(
        "nhtj,nhji->nhti", reads[..., :HEAD_CHANNELS], jnp.stack(starts)
    )
    merged_output = merged_output.transpose(0, 2, 1, 3).reshape(
        row_count, head_count, HEAD_CHANNELS
    )
    mixer_result = complete_head_outputs(
        merged_output,
        receptance_rows,
        key_row_block,
        value_row_block,
        head_norm_gain,
        self_key_weight,
        mixer_output_gate,
    )
    return lax.psum_scatter(
        jnp.dot(mixer_result, mixer_output_weight, preferred_element_type=jnp.float32).astype(
            jnp.bfloat16
        ),
        "tp",
        scatter_dimension=0,
        tiled=True,
    )


def activate(rows_in, gate_part, up_part):
    pre_gate = jnp.einsum("fd,rd->fr", gate_part, rows_in, preferred_element_type=jnp.float32)
    pre_up = jnp.einsum("fd,rd->fr", up_part, rows_in, preferred_element_type=jnp.float32)
    return (jax.nn.silu(pre_gate) * pre_up).astype(jnp.bfloat16)


def expert_entry(
    second_batch_rows,
    routed_expert_index,
    routing_output_weight,
    expert_norm_gain,
    common_expert_gate,
    common_expert_up,
):
    row_count, width = second_batch_rows.shape
    top_count = routed_expert_index.shape[1]
    peer_count = lax.axis_size("ep")
    slot_count = 3 * row_count * top_count // (2 * peer_count)
    widened = second_batch_rows.astype(jnp.float32)
    normalized_rows = (
        widened
        * lax.rsqrt(jnp.mean(widened * widened, axis=-1, keepdims=True) + NORM_FLOOR)
        * expert_norm_gain
    ).astype(jnp.bfloat16)
    flat_ids = routed_expert_index.reshape(-1)
    one_hot = (flat_ids[:, None] == jnp.arange(peer_count, dtype=jnp.int32)[None, :]).astype(
        jnp.int32
    )
    slot_rank = jnp.sum((jnp.cumsum(one_hot, axis=0) - 1) * one_hot, axis=1)
    target = flat_ids * slot_count + slot_rank
    owners = jnp.arange(row_count * top_count, dtype=jnp.int32) // top_count
    source_row = jnp.full((peer_count * slot_count,), row_count, jnp.int32).at[target].set(owners)
    padded = jnp.concatenate([normalized_rows, jnp.zeros((1, width), jnp.bfloat16)], axis=0)
    outgoing = jnp.take(padded, source_row, axis=0).reshape(peer_count, slot_count, width)
    shared_hidden = activate(normalized_rows, common_expert_gate, common_expert_up)
    piece_width = width // lax.axis_size("tp")
    own_slice = lax.dynamic_slice_in_dim(
        outgoing, lax.axis_index("tp") * piece_width, piece_width, 2
    )
    arrived = lax.all_to_all(own_slice, "ep", split_axis=0, concat_axis=0, tiled=True)
    return (arrived, shared_hidden, target)


def expert_exit(
    arrived,
    shared_hidden,
    target,
    routing_output_weight,
    expert_gate_weight,
    expert_up_weight,
    expert_down_weight,
    common_expert_down,
):
    peer_count, slot_count, piece_width = arrived.shape
    row_count, top_count = routing_output_weight.shape
    out_width = expert_down_weight.shape[2]
    flat_rows = arrived.reshape(-1, piece_width)
    pieces = lax.all_gather(flat_rows, "tp", axis=1, tiled=True)
    gate_cols = expert_gate_weight[0]
    up_cols = expert_up_weight[0]
    pre_gate = jnp.einsum("fd,rd->fr", gate_cols, pieces, preferred_element_type=jnp.float32)
    pre_up = jnp.einsum("fd,rd->fr", up_cols, pieces, preferred_element_type=jnp.float32)
    routed_hidden = (jax.nn.silu(pre_gate) * pre_up).astype(jnp.bfloat16)
    both = lax.all_gather(
        jnp.concatenate([routed_hidden, shared_hidden], axis=1), "tp", axis=0, tiled=True
    )
    pieces = (both[:, : routed_hidden.shape[1]], both[:, routed_hidden.shape[1] :])
    routed_rows = expert_down_weight[0]
    routed_sum = jnp.einsum("fr,fd->rd", pieces[0], routed_rows, preferred_element_type=jnp.float32)
    shared_out = jnp.einsum(
        "fr,fd->rd", pieces[1], common_expert_down, preferred_element_type=jnp.float32
    )
    returned = lax.all_to_all(
        routed_sum.astype(jnp.bfloat16).reshape(peer_count, slot_count, out_width),
        "ep",
        split_axis=0,
        concat_axis=0,
        tiled=True,
    )
    picked = jnp.take(returned.reshape(-1, out_width), target, axis=0).reshape(
        row_count, top_count, out_width
    )
    merged_output = (
        jnp.sum(picked.astype(jnp.float32) * routing_output_weight[:, :, None], axis=1) + shared_out
    )
    return merged_output.astype(jnp.bfloat16)


def on_device(
    receptance,
    key_tensor,
    value_tensor,
    decay_data_input,
    correction_rate_input,
    mixer_output_gate,
    decay_channel_offset,
    head_norm_gain,
    self_key_weight,
    mixer_output_weight,
    second_batch_rows,
    routed_expert_index,
    routing_output_weight,
    expert_norm_gain,
    expert_gate_weight,
    expert_up_weight,
    expert_down_weight,
    common_expert_gate,
    common_expert_up,
    common_expert_down,
):
    arrived, shared_hidden, target = expert_entry(
        second_batch_rows,
        routed_expert_index,
        routing_output_weight,
        expert_norm_gain,
        common_expert_gate,
        common_expert_up,
    )
    arrived, receptance, key_tensor, value_tensor, decay_data_input, correction_rate_input = (
        lax.optimization_barrier(
            (arrived, receptance, key_tensor, value_tensor, decay_data_input, correction_rate_input)
        )
    )
    token_mixer_output = mixer_part(
        receptance,
        key_tensor,
        value_tensor,
        decay_data_input,
        correction_rate_input,
        mixer_output_gate,
        decay_channel_offset,
        head_norm_gain,
        self_key_weight,
        mixer_output_weight,
    )
    expert_out = expert_exit(
        arrived,
        shared_hidden,
        target,
        routing_output_weight,
        expert_gate_weight,
        expert_up_weight,
        expert_down_weight,
        common_expert_down,
    )
    return (token_mixer_output, expert_out)


def solution(mesh):
    in_specs = (
        P("ep", "tp"),
        P("ep", "tp"),
        P("ep", "tp"),
        P("ep", "tp"),
        P("ep", "tp"),
        P("ep", "tp"),
        P("tp"),
        P("tp"),
        P("tp"),
        P("tp", None),
        P("ep", None),
        P("ep", None),
        P("ep", None),
        P(),
        P("ep", "tp", None),
        P("ep", "tp", None),
        P("ep", None, "tp"),
        P("tp", None),
        P("tp", None),
        P(None, "tp"),
    )
    out_specs = (P(("ep", "tp"), None), P("ep", "tp"))
    return jax.shard_map(
        on_device, mesh=mesh, in_specs=in_specs, out_specs=out_specs, check_vma=False
    )
```

profile of v0, /device:TPU:0, one launch (start us, length us, event | category | flops | bytes accessed | tf_op | source)
XLA Modules:
  0.0 244.3 jit_solution(18401035282546436214)
XLA Ops:
  9.3 1.1 reduce-window.6
  10.8 2.4 %scatter_custom_fusion = s32[768]{0:T(1024)S(1)} fusion(s32[512]{0:T(512)S(1)} %bitcast.192, s32[512]{0:T(512)S(1)} %add_select_fusion, s32[]{:T(128)} %constant.328.clone.1), kind=kCustom, calls=%fused_computation.208 | custom fusion | bytes 3076 | tf_op jit(solution)/shard_map/scatter | solution.py:214
  13.3 1.2 fusion.32
  14.6 1.2 fusion.34
  16.7 4.3 %gather_fusion = bf16[768,2048]{1,0:T(8,128)(2,1)} fusion(bf16[129,2048]{1,0:T(8,128)(2,1)S(1)} %concatenate.33, s32[1024]{0:T(1024)S(1)} %pad_clamp_fusion.1), kind=kCustom, calls=%fused_computation | custom fusion | bytes 6294528 | tf_op jit(solution)/shard_map/jit(_take)/gather | solution.py:216
  20.9 2.3 dynamic-slice_select_fusion
  23.2 6.4 %all-to-all-start = ((bf16[8,96,512]{2,1,0:T(8,128)(2,1)}), bf16[8,96,512]{2,1,0:T(8,128)(2,1)S(1)}, u32[]{:S(2)}, u32[]{:S(2)}) async-start(bf16[8,96,512]{2,1,0:T(8,128)(2,1)} %dynamic-slice_select_fusion), calls=%async_computation | async-start | bytes 1572864 | tf_op jit(solution)/shard_map/all_to_all | solution.py:222
  30.5 20.0 %all-to-all-done = bf16[8,96,512]{2,1,0:T(8,128)(2,1)S(1)} async-done(((bf16[8,96,512]{2,1,0:T(8,128)(2,1)}), bf16[8,96,512]{2,1,0:T(8,128)(2,1)S(1)}, u32[]{:S(2)}, u32[]{:S(2)}) %all-to-all-start) | async-done | bytes 786464 | tf_op jit(solution)/shard_map/all_to_all | solution.py:222
  50.7 1.9 copy.246
  52.6 2.3 add_divide_fusion
  54.9 2.2 reshape.842
  57.1 1.4 reshape.885
  58.6 1.6 copy.252
  60.5 2.2 reshape.834
  62.7 2.4 reshape.884
  65.1 2.6 %copy.248 = f32[4,64,8,64]{3,1,2,0:T(8,128)} copy(f32[4,64,8,64]{1,0,3,2:T(4,128)} %reshape.884) | data formatting | bytes 1048576 | tf_op jit(solution)/shard_map/reshape | solution.py:95
  67.7 5.0 %fusion.67 = (f32[4,8,64,64]{3,2,1,0:T(8,128)S(1)}, f32[4,8,64,64]{3,2,1,0:T(8,128)S(1)}, f32[4,8,64,64]{3,2,1,0:T(8,128)S(1)}, f32[4,8,64,64]{3,2,1,0:T(8,128)S(1)}, f32[4,8,64,64]{3,2,1,0:T(8,128)}) fusion(f32[4,64,8,64]{3,2,1,0:T(8,128)} %reshape.842, f32[4,8,64]{2,1,0:T(8,128)S(1)} %add_rsqrt_fusion.1, f32[4,64,8,64]{3,1,2,0:T(8,128)S(1)} %copy.252, ...), kind=kOutput, calls=%fused_computation.114 | convolution fusion | flops 101715968 | bytes 4726784 | tf_op jit(solution)/shard_map/ts,nhsd->nhtd/dot_general | solution.py:105
  72.7 2.3 fusion.1
  82.6 1.6 convolution_subtract_fusion
  84.3 1.6 slice_select_fusion.4
  85.9 2.1 reshape.836
  87.9 2.5 %fusion.8 = f32[4,8,128,64]{3,2,1,0:T(8,128)S(1)} fusion(f32[4,8,64,64]{3,2,1,0:T(8,128)} %get-tuple-element.19, f32[4,8,64,64]{3,2,1,0:T(8,128)} %get-tuple-element.18, bf16[4,8,64,64]{3,1,2,0:T(8,128)(2,1)} %bitcast.178), kind=kOutput, calls=%fused_computation.12 | convolution fusion | flops 100925440 | bytes 2359296 | tf_op jit(solution)/shard_map/nhts,nhsd->nhtd/dot_general | solution.py:47
  90.4 1.1 fusion.129
  94.9 1.7 convolution_subtract_fusion.5
  99.6 1.7 convolution_bitcast_fusion.4
  101.3 2.0 fusion.31
  105.2 2.0 copy.274
  107.3 3.7 %convolution_subtract_fusion.6 = f32[4,8,64,128]{3,2,1,0:T(8,128)} fusion(f32[4,8,64,128]{3,2,1,0:T(8,128)} %copy-done.8, f32[4,8,128,128]{3,2,1,0:T(8,128)} %copy-done.1, f32[4,8,64,64]{3,2,1,0:T(8,128)} %get-tuple-element.16, f32[4,8,64,64]{3,2,1,0:T(8,128)S(1)} %copy-done.7, pred[64,64]{1,0:T(8,128)(4,1)S(1)} %iota_compare_fusion.2), kind=kOutput, calls=%fused_computation.27 | convolution fusion | flops 101318656 | bytes 4722688 | tf_op jit(solution)/shard_map/nhts,nhsd->nhtd/dot_general | solution.py:47
  111.0 9.0 %all-gather.9.cloned.1.call-done = bf16[64,64,128]{2,1,0:T(8,128)(2,1)} async-done(((bf16[8,64,128]{2,1,0:T(8,128)(2,1)}), bf16[64,64,128]{2,1,0:T(8,128)(2,1)}) %all-gather.9.cloned.1.call-update) | async-done | bytes 1048592 | tf_op jit(solution)/shard_map/all_gather | solution.py:144
  120.0 1.2 fusion.27
  121.2 1.2 fusion.26
  122.4 1.2 fusion.25
  123.6 41.5 %all-gather.5.cloned.1.call-done = bf16[768,2048]{1,0:T(8,128)(2,1)} async-done(((bf16[768,512]{1,0:T(8,128)(2,1)}), bf16[768,2048]{1,0:T(8,128)(2,1)}) %all-gather.5.cloned.1.call-update) | async-done | bytes 3145744 | tf_op jit(solution)/shard_map/all_gather | solution.py:240
  165.1 3.3 %convolution_bitcast_fusion.2 = f32[256,768]{0,1:T(8,128)S(1)} fusion(bf16[768,2048]{1,0:T(8,128)(2,1)} %all-gather.5.cloned.1.call-done, bf16[1,256,2048]{2,1,0:T(8,128)(2,1)} %param.34), kind=kOutput, calls=%fused_computation.32 | convolution fusion | flops 805306368 | bytes 4980736 | tf_op jit(solution)/shard_map/fd,rd->fr/dot_general | solution.py:243
  168.5 1.0 fusion.19
  170.7 1.2 fusion.24
  171.9 1.3 fusion.23
  173.2 1.2 fusion.22
  174.4 1.2 fusion.21
  179.6 2.1 copy.273
  181.7 1.1 reshape.837
  183.1 3.2 %convolution_convert_fusion = bf16[256,2048]{1,0:T(8,128)(2,1)} fusion(bf16[512,2048]{1,0:T(8,128)(2,1)S(1)} %copy-done, bf16[256,512]{1,0:T(8,128)(2,1)} %param.25, f32[256,512]{1,0:T(8,128)} %copy.274, bf16[256,512]{1,0:T(8,128)(2,1)S(1)} %copy-done.17, f32[256,512]{1,0:T(8,128)} %copy.273, f32[256,512]{1,0:T(8,128)} %reshape.837, ...), kind=kOutput, calls=%fused_computation.4 | convolution fusion | flops 538574848 | bytes 5769216 | tf_op jit(solution)/shard_map/dot_general | solution.py:174
  186.4 17.0 %all-gather.7.cloned.1.call-done = bf16[1024,896]{0,1:T(8,128)(2,1)} async-done(((bf16[256,896]{0,1:T(8,128)(2,1)}), bf16[1024,896]{0,1:T(8,128)(2,1)}) %all-gather.7.cloned.1.call-update) | async-done | bytes 1835024 | tf_op jit(solution)/shard_map/all_gather | solution.py:246
  203.4 3.5 %fusion.14 = bf16[768,512]{1,0:T(8,128)(2,1)} fusion(bf16[1024,896]{0,1:T(8,128)(2,1)} %all-gather.7.cloned.1.call-done, bf16[1,1024,512]{2,1,0:T(8,128)(2,1)} %param.36), kind=kOutput, calls=%fused_computation.23 | convolution fusion | flops 805699584 | bytes 3407872 | tf_op jit(solution)/shard_map/fr,fd->rd/dot_general | solution.py:251
  207.0 4.6 %all-to-all-start.1 = ((bf16[8,96,512]{2,1,0:T(8,128)(2,1)}), bf16[8,96,512]{2,1,0:T(8,128)(2,1)S(1)}, u32[]{:S(2)}, u32[]{:S(2)}) async-start(bf16[8,96,512]{2,1,0:T(8,128)(2,1)} %bitcast.187), calls=%async_computation.2 | async-start | bytes 1572864 | tf_op jit(solution)/shard_map/all_to_all | solution.py:255
  212.0 20.5 %all-to-all-done.1 = bf16[8,96,512]{2,1,0:T(8,128)(2,1)S(1)} async-done(((bf16[8,96,512]{2,1,0:T(8,128)(2,1)}), bf16[8,96,512]{2,1,0:T(8,128)(2,1)S(1)}, u32[]{:S(2)}, u32[]{:S(2)}) %all-to-all-start.1) | async-done | bytes 786464 | tf_op jit(solution)/shard_map/all_to_all | solution.py:255
  232.5 2.0 gather_fusion.1
  235.5 2.3 fusion.29
  (147 shorter events, 27.1 us)
Async XLA Ops:
  7.2 175.9 %copy-start = (bf16[512,2048]{1,0:T(8,128)(2,1)S(1)}, bf16[512,2048]{1,0:T(8,128)(2,1)}, u32[]{:S(2)}) copy-start(bf16[512,2048]{1,0:T(8,128)(2,1)} %param.29) | copy-start | bytes 6291460
  15.8 0.8 copy-start.12
  20.9 29.6 %copy-start.18 = (bf16[256,512]{1,0:T(8,128)(2,1)S(1)}, bf16[256,512]{1,0:T(8,128)(2,1)}, u32[]{:S(2)}) copy-start(bf16[256,512]{1,0:T(8,128)(2,1)} %param.21) | copy-start | bytes 786436
  20.9 31.7 %copy-start.20 = (f32[512]{0:T(512)S(1)}, f32[512]{0:T(512)}, u32[]{:S(2)}) copy-start(f32[512]{0:T(512)} %param.26) | copy-start | bytes 6148
  23.2 27.3 %all-to-all-start = ((bf16[8,96,512]{2,1,0:T(8,128)(2,1)}), bf16[8,96,512]{2,1,0:T(8,128)(2,1)S(1)}, u32[]{:S(2)}, u32[]{:S(2)}) async-start(bf16[8,96,512]{2,1,0:T(8,128)(2,1)} %dynamic-slice_select_fusion), calls=%async_computation | async-start | bytes 1572864 | tf_op jit(solution)/shard_map/all_to_all | solution.py:222
  29.6 90.4 %all-gather.9.cloned.1.call-start = ((), (), s32[]{:S(2)}) async-start(), calls=%async_computation.6 | async-start | bytes 1179648 | tf_op jit(solution)/shard_map/all_gather | solution.py:144
  50.5 6.6 %copy-start.16 = (bf16[8,96,512]{2,1,0:T(8,128)(2,1)}, bf16[8,96,512]{2,1,0:T(8,128)(2,1)S(1)}, u32[]{:S(2)}) copy-start(bf16[8,96,512]{2,1,0:T(8,128)(2,1)S(1)} %all-to-all-done) | copy-start | bytes 2359300
  72.7 2.3 copy-start.6
  72.7 2.3 copy-start.9
  75.1 9.2 %copy-start.1 = (f32[4,8,128,128]{3,2,1,0:T(8,128)}, f32[4,8,128,128]{3,2,1,0:T(8,128)S(1)}, u32[]{:S(2)}) copy-start(f32[4,8,128,128]{3,2,1,0:T(8,128)S(1)} %fusion.1) | copy-start | bytes 6291460
  90.4 1.6 copy-start.4
  90.4 1.7 copy-start.11
  92.2 1.2 copy-start.10
  92.2 1.5 copy-start.15
  93.7 1.2 copy-start.5
  94.9 1.8 copy-start.8
  96.7 1.1 copy-start.2
  97.0 2.5 %copy-start.22 = (f32[512]{0:T(512)S(1)}, f32[512]{0:T(512)}, u32[]{:S(2)}) copy-start(f32[512]{0:T(512)} %param.28) | copy-start | bytes 6148
  97.0 2.6 %copy-start.13 = (bf16[128,2048]{1,0:T(8,128)(2,1)S(1)}, bf16[128,2048]{1,0:T(8,128)(2,1)}, u32[]{:S(2)}) copy-start(bf16[128,2048]{1,0:T(8,128)(2,1)} %copy-done.12) | copy-start | bytes 1572868
  98.7 66.4 %all-gather.5.cloned.1.call-start = ((), (), s32[]{:S(2)}) async-start(), calls=%async_computation.4 | async-start | bytes 3932160 | tf_op jit(solution)/shard_map/all_gather | solution.py:240
  99.4 104.0 %all-gather.7.cloned.1.call-start = ((), (), s32[]{:S(2)}) async-start(), calls=%async_computation.5 | async-start | bytes 2293760 | tf_op jit(solution)/shard_map/all_gather | solution.py:246
  101.3 6.0 %copy-start.7 = (f32[4,8,64,64]{3,2,1,0:T(8,128)S(1)}, f32[4,8,64,64]{3,2,1,0:T(8,128)}, u32[]{:S(2)}) copy-start(f32[4,8,64,64]{3,2,1,0:T(8,128)} %copy-done.6) | copy-start | bytes 1572868
  123.6 44.9 %copy-start.25 = (bf16[1,256,2048]{2,1,0:T(8,128)(2,1)S(1)}, bf16[1,256,2048]{2,1,0:T(8,128)(2,1)}, u32[]{:S(2)}) copy-start(bf16[1,256,2048]{2,1,0:T(8,128)(2,1)} %param.35) | copy-start | bytes 3145732
  165.1 3.4 %copy-start.24 = (bf16[768,2048]{1,0:T(8,128)(2,1)S(1)}, bf16[768,2048]{1,0:T(8,128)(2,1)}, u32[]{:S(2)}) copy-start(bf16[768,2048]{1,0:T(8,128)(2,1)} %all-gather.5.cloned.1.call-done) | copy-start | bytes 9437188
  169.5 6.1 %copy-start.3 = (f32[4,8,64,128]{3,2,1,0:T(8,128)S(1)}, f32[4,8,64,128]{3,2,1,0:T(8,128)}, u32[]{:S(2)}) copy-start(f32[4,8,64,128]{3,2,1,0:T(8,128)} %copy-done.2) | copy-start | bytes 3145732
  170.4 67.4 %reduce-scatter.2.cloned.1.call-start = ((), (), s32[]{:S(2)}) async-start(), calls=%async_computation.3 | async-start | bytes 1310720 | tf_op jit(solution)/shard_map/reduce_scatter | solution.py:173
  171.9 4.5 %copy-start.14 = (f32[4,8,64,128]{3,2,1,0:T(8,128)S(1)}, f32[4,8,64,128]{3,2,1,0:T(8,128)}, u32[]{:S(2)}) copy-start(f32[4,8,64,128]{3,2,1,0:T(8,128)} %convolution_subtract_fusion.6) | copy-start | bytes 3145732
  179.6 3.5 %copy-start.17 = (bf16[256,512]{1,0:T(8,128)(2,1)S(1)}, bf16[256,512]{1,0:T(8,128)(2,1)}, u32[]{:S(2)}) copy-start(bf16[256,512]{1,0:T(8,128)(2,1)} %param.22) | copy-start | bytes 786436
  179.6 3.5 %copy-start.21 = (f32[512]{0:T(512)S(1)}, f32[512]{0:T(512)}, u32[]{:S(2)}) copy-start(f32[512]{0:T(512)} %param.27) | copy-start | bytes 6148
  186.4 25.3 %copy-start.23 = (f32[128,4]{0,1:T(4,128)S(1)}, f32[128,4]{0,1:T(4,128)}, u32[]{:S(2)}) copy-start(f32[128,4]{0,1:T(4,128)} %param.32) | copy-start | bytes 6148
  186.4 25.5 %copy-start.19 = (s32[128,4]{0,1:T(4,128)S(1)}, s32[128,4]{0,1:T(4,128)}, u32[]{:S(2)}) copy-start(s32[128,4]{0,1:T(4,128)} %param.31) | copy-start | bytes 6148
  207.0 25.6 %all-to-all-start.1 = ((bf16[8,96,512]{2,1,0:T(8,128)(2,1)}), bf16[8,96,512]{2,1,0:T(8,128)(2,1)S(1)}, u32[]{:S(2)}, u32[]{:S(2)}) async-start(bf16[8,96,512]{2,1,0:T(8,128)(2,1)} %bitcast.187), calls=%async_computation.2 | async-start | bytes 1572864 | tf_op jit(solution)/shard_map/all_to_all | solution.py:255
Sparse Core Ops, SparseCore 0:
  98.8 21.1 all-gather.8
  121.8 43.2 all-gather.4
  170.5 32.8 all-gather.6
  206.7 27.9 reduce-scatter.1
where the time goes:
time: 246 us; the launch traced here: 244 us
  waiting for transfers between devices  109 us (44%)
  matrix products  54.7 us (22%)
  local copies, waits for them, and re-layouts  38.5 us (16%)
  other arithmetic  16.2 us (7%)
  between operations  14.6 us (6%)
  starting transfers between devices  11.6 us (5%)
    all_gather x1, waiting for transfers between devices, expert_exit(): pieces = lax.all_gather(flat_rows, 'tp', axis=1, tiled=True)  41.5 us
    dot_general x30, matrix products, product(): jnp.einsum(spec, left, right, precision=PRECISION, preferred_element_type...  32.6 us
    all_to_all x1, waiting for transfers between devices, expert_exit(): lax.all_to_all(routed_sum.astype(jnp.bfloat16).reshape(peer_count, slot_c...  20.5 us
    all_to_all x1, waiting for transfers between devices, expert_entry(): lax.all_to_all(own_slice, 'ep', split_axis=0, concat_axis=0, tiled=True)  20 us
    all_gather x1, waiting for transfers between devices, expert_exit(): lax.all_gather(jnp.concatenate([routed_hidden, shared_hidden], axis=1), '...  17 us
    reshape x6, local copies, waits for them, and re-layouts, by_block(): return matrix.astype(jnp.float32).reshape(block_count, span, head_count,...  12.3 us
    all_gather x1, waiting for transfers between devices, mixer_part(): everything = lax.all_gather(whole.astype(jnp.bfloat16), 'ep')  9.03 us
    all_to_all x1, starting transfers between devices, expert_entry(): lax.all_to_all(own_slice, 'ep', split_axis=0, concat_axis=0, tiled=True)  6.35 us
  transfers between devices with their start and end apart: 6, of which 5 were waited for; matrix products, arithmetic and copies ran while one was open for 17% of the time, Pallas kernels for 0%

commit v1 on v0

--- a/solution.py
+++ b/solution.py
@@ -237,7 +237,15 @@
     row_count, top_count = routing_output_weight.shape
     out_width = expert_down_weight.shape[2]
     flat_rows = arrived.reshape(-1, piece_width)
-    pieces = lax.all_gather(flat_rows, "tp", axis=1, tiled=True)
+    cores_n = lax.axis_size("tp")
+    f_now = sorted(((u, (u + 1) % cores_n) for u in range(cores_n)))
+    u1 = flat_rows
+    pool = [u1]
+    for j0 in range(1, cores_n):
+        u1 = lax.ppermute(u1, axis_name="tp", perm=f_now)
+        pool.insert(0, u1)
+    finding = jnp.concatenate(pool, axis=1)
+    pieces = jnp.roll(finding, (lax.axis_index("tp") + 1) * flat_rows.shape[1], axis=1)
     gate_cols = expert_gate_weight[0]
     up_cols = expert_up_weight[0]
     pre_gate = jnp.einsum("fd,rd->fr", gate_cols, pieces, preferred_element_type=jnp.float32)

time: 246 us -> 241 us (0.980)
  waiting for transfers between devices: 109 us -> 98.1 us
  local copies, waits for them, and re-layouts: 38.5 us -> 43.7 us
  matrix products: 54.7 us -> 51.7 us
    all_gather x1 -> x0, waiting for transfers between devices: 41.5 us -> none  [expert_exit(): pieces = lax.all_gather(flat_rows, 'tp', axis=1, tiled=True)]
    ppermute x0 -> x3, waiting for transfers between devices: none -> 41.1 us  [expert_exit(): u1 = lax.ppermute(u1, axis_name='tp', perm=f_now)]
    all_gather x1, waiting for transfers between devices: 9.03 us -> 0.01 us  [mixer_part(): everything = lax.all_gather(whole.astype(jnp.bfloat16), 'ep')]
    unnamed x54 -> x73, local copies, waits for them, and re-layouts: 3.55 us -> 12.1 us
  transfers between devices with their start and end apart: 6 -> 8, of which waited for: 5 -> 6; matrix products, arithmetic and copies ran while one was open for 17% -> 17% of each run, Pallas kernels for 0% -> 0%
where the time goes in v1:
time: 241 us; the launch traced here: 240 us
  waiting for transfers between devices  98.1 us (41%)
  matrix products  51.7 us (21%)
  local copies, waits for them, and re-layouts  43.7 us (18%)
  between operations  16.4 us (7%)
  other arithmetic  16.2 us (7%)
  starting transfers between devices  13.6 us (6%)
    ppermute x3, waiting for transfers between devices, expert_exit(): u1 = lax.ppermute(u1, axis_name='tp', perm=f_now)  41.1 us
    dot_general x30, matrix products, product(): jnp.einsum(spec, left, right, precision=PRECISION, preferred_element_type...  32 us
    all_to_all x1, waiting for transfers between devices, expert_exit(): lax.all_to_all(routed_sum.astype(jnp.bfloat16).reshape(peer_count, slot_c...  20.5 us
    all_to_all x1, waiting for transfers between devices, expert_entry(): lax.all_to_all(own_slice, 'ep', split_axis=0, concat_axis=0, tiled=True)  20 us
    all_gather x1, waiting for transfers between devices, expert_exit(): lax.all_gather(jnp.concatenate([routed_hidden, shared_hidden], axis=1), '...  16.4 us
    unnamed x73, local copies, waits for them, and re-layouts  12.1 us
    reshape x6, local copies, waits for them, and re-layouts, by_block(): return matrix.astype(jnp.float32).reshape(block_count, span, head_count,...  10.3 us
    all_to_all x1, starting transfers between devices, expert_entry(): lax.all_to_all(own_slice, 'ep', split_axis=0, concat_axis=0, tiled=True)  6.35 us
  transfers between devices with their start and end apart: 8, of which 6 were waited for; matrix products, arithmetic and copies ran while one was open for 17% of the time, Pallas kernels for 0%

profile of v1, /device:TPU:0, one launch (start us, length us, event | category | flops | bytes accessed | tf_op | source)
XLA Modules:
  0.0 239.7 jit_solution(8954415010661315971)
XLA Ops:
  11.6 2.4 %scatter_custom_fusion = s32[768]{0:T(1024)S(1)} fusion(s32[512]{0:T(512)S(1)} %bitcast.192, s32[512]{0:T(512)S(1)} %add_select_fusion, s32[]{:T(128)} %constant.346.clone.1), kind=kCustom, calls=%fused_computation.219 | custom fusion | bytes 3076 | tf_op jit(solution)/shard_map/scatter | solution.py:214
  14.1 1.2 fusion.40
  15.4 1.2 fusion.42
  17.5 4.3 %gather_fusion = bf16[768,2048]{1,0:T(8,128)(2,1)} fusion(bf16[129,2048]{1,0:T(8,128)(2,1)S(1)} %concatenate.39, s32[1024]{0:T(1024)S(1)} %pad_clamp_fusion.1), kind=kCustom, calls=%fused_computation | custom fusion | bytes 6294528 | tf_op jit(solution)/shard_map/jit(_take)/gather | solution.py:216
  21.8 2.3 dynamic-slice_select_fusion
  24.1 6.4 %all-to-all-start = ((bf16[8,96,512]{2,1,0:T(8,128)(2,1)}), bf16[8,96,512]{2,1,0:T(8,128)(2,1)S(1)}, u32[]{:S(2)}, u32[]{:S(2)}) async-start(bf16[8,96,512]{2,1,0:T(8,128)(2,1)} %dynamic-slice_select_fusion), calls=%async_computation | async-start | bytes 1572864 | tf_op jit(solution)/shard_map/all_to_all | solution.py:222
  31.4 20.0 %all-to-all-done = bf16[8,96,512]{2,1,0:T(8,128)(2,1)S(1)} async-done(((bf16[8,96,512]{2,1,0:T(8,128)(2,1)}), bf16[8,96,512]{2,1,0:T(8,128)(2,1)S(1)}, u32[]{:S(2)}, u32[]{:S(2)}) %all-to-all-start) | async-done | bytes 786464 | tf_op jit(solution)/shard_map/all_to_all | solution.py:222
  51.5 1.3 copy.246
  52.9 2.4 %add_divide_fusion = (f32[256,512]{1,0:T(8,128)}, f32[256,512]{1,0:T(8,128)}) fusion(bf16[256,512]{1,0:T(8,128)(2,1)} %param.24, bf16[256,512]{1,0:T(8,128)(2,1)} %param.23, f32[512]{0:T(512)S(1)} %copy-done.26), kind=kLoop, calls=%fused_computation.137 | loop fusion | flops 1310720 | bytes 1574912 | tf_op jit(solution)/shard_map/div | solution.py:108
  55.3 2.2 reshape.842
  57.5 1.4 reshape.885
  59.0 1.6 copy.252
  60.9 2.2 reshape.834
  63.1 1.4 reshape.884
  64.6 2.6 %copy.248 = f32[4,64,8,64]{3,1,2,0:T(8,128)} copy(f32[4,64,8,64]{1,0,3,2:T(4,128)} %reshape.884) | data formatting | bytes 1048576 | tf_op jit(solution)/shard_map/reshape | solution.py:95
  67.2 5.0 %fusion.75 = (f32[4,8,64,64]{3,2,1,0:T(8,128)S(1)}, f32[4,8,64,64]{3,2,1,0:T(8,128)S(1)}, f32[4,8,64,64]{3,2,1,0:T(8,128)S(1)}, f32[4,8,64,64]{3,2,1,0:T(8,128)S(1)}, f32[4,8,64,64]{3,2,1,0:T(8,128)}) fusion(f32[4,64,8,64]{3,2,1,0:T(8,128)} %reshape.842, f32[4,8,64]{2,1,0:T(8,128)S(1)} %add_rsqrt_fusion.1, f32[4,64,8,64]{3,1,2,0:T(8,128)S(1)} %copy.252, ...), kind=kOutput, calls=%fused_computation.116 | convolution fusion | flops 101715968 | bytes 4726784 | tf_op jit(solution)/shard_map/ts,nhsd->nhtd/dot_general | solution.py:105
  72.1 2.3 fusion.5
  82.0 1.6 convolution_subtract_fusion
  83.6 1.7 slice_select_fusion.4
  86.4 2.5 %fusion.12 = f32[4,8,128,64]{3,2,1,0:T(8,128)S(1)} fusion(f32[4,8,64,64]{3,2,1,0:T(8,128)} %get-tuple-element.19, f32[4,8,64,64]{3,2,1,0:T(8,128)} %get-tuple-element.18, bf16[4,8,64,64]{3,1,2,0:T(8,128)(2,1)} %bitcast.179), kind=kOutput, calls=%fused_computation.16 | convolution fusion | flops 100925440 | bytes 2359296 | tf_op jit(solution)/shard_map/nhts,nhsd->nhtd/dot_general | solution.py:47
  93.3 1.7 convolution_subtract_fusion.5
  96.6 1.5 collective-permute-start
  99.5 1.9 convolution_bitcast_fusion.2
  101.4 15.2 %collective-permute-done = bf16[768,512]{1,0:T(8,128)(2,1)} collective-permute-done((bf16[768,512]{1,0:T(8,128)(2,1)S(1)}, bf16[768,512]{1,0:T(8,128)(2,1)}, u32[]{:S(2)}, u32[]{:S(2)}) %collective-permute-start) | collective-permute-done | bytes 786464 | tf_op jit(solution)/shard_map/ppermute | solution.py:245
  117.2 1.7 fusion.39
  120.1 3.2 %convolution_subtract_fusion.6 = f32[4,8,64,128]{3,2,1,0:T(8,128)} fusion(f32[4,8,64,128]{3,2,1,0:T(8,128)S(1)} %copy-done.10, f32[4,8,128,128]{3,2,1,0:T(8,128)S(1)} %copy-done.2, f32[4,8,64,64]{3,2,1,0:T(8,128)} %get-tuple-element.16, f32[4,8,64,64]{3,2,1,0:T(8,128)S(1)} %copy-done.8, pred[64,64]{1,0:T(8,128)(4,1)S(1)} %iota_compare_fusion.2), kind=kOutput, calls=%fused_computation.31 | convolution fusion | flops 101318656 | bytes 4726784 | tf_op jit(solution)/shard_map/nhts,nhsd->nhtd/dot_general | solution.py:47
  123.2 12.7 %collective-permute-done.1 = bf16[768,512]{1,0:T(8,128)(2,1)} collective-permute-done((bf16[768,512]{1,0:T(8,128)(2,1)}, bf16[768,512]{1,0:T(8,128)(2,1)}, u32[]{:S(2)}, u32[]{:S(2)}) %collective-permute-start.1) | collective-permute-done | bytes 786464 | tf_op jit(solution)/shard_map/ppermute | solution.py:245
  138.9 1.2 fusion.34
  140.2 1.2 fusion.33
  141.4 13.1 %collective-permute-done.2 = bf16[768,512]{1,0:T(8,128)(2,1)} collective-permute-done((bf16[768,512]{1,0:T(8,128)(2,1)}, bf16[768,512]{1,0:T(8,128)(2,1)}, u32[]{:S(2)}, u32[]{:S(2)}) %collective-permute-start.2) | collective-permute-done | bytes 786464 | tf_op jit(solution)/shard_map/ppermute | solution.py:245
  154.5 1.2 constant_dynamic-update-slice_fusion.7
  155.7 1.2 constant_dynamic-update-slice_fusion.6
  157.0 1.2 constant_dynamic-update-slice_fusion.5
  158.3 1.2 constant_dynamic-update-slice_fusion.3
  159.6 1.3 constant_dynamic-update-slice_fusion.2
  160.9 1.2 constant_dynamic-update-slice_fusion.1
  165.7 1.2 fusion.32
  166.9 1.3 fusion.31
  168.2 1.2 fusion.30
  169.4 1.2 fusion.29
  174.7 2.1 copy.273
  178.2 3.2 %convolution_convert_fusion = bf16[256,2048]{1,0:T(8,128)(2,1)} fusion(bf16[512,2048]{1,0:T(8,128)(2,1)S(1)} %copy-done, bf16[256,512]{1,0:T(8,128)(2,1)} %param.25, f32[256,512]{1,0:T(8,128)} %copy.274, bf16[256,512]{1,0:T(8,128)(2,1)S(1)} %copy-done.23, f32[256,512]{1,0:T(8,128)} %copy.273, f32[256,512]{1,0:T(8,128)} %reshape.837, ...), kind=kOutput, calls=%fused_computation.8 | convolution fusion | flops 538574848 | bytes 5769216 | tf_op jit(solution)/shard_map/dot_general | solution.py:174
  181.4 16.4 %all-gather.4.cloned.1.call-done = bf16[1024,896]{0,1:T(8,128)(2,1)} async-done(((bf16[256,896]{0,1:T(8,128)(2,1)}), bf16[1024,896]{0,1:T(8,128)(2,1)}) %all-gather.4.cloned.1.call-update) | async-done | bytes 1835024 | tf_op jit(solution)/shard_map/all_gather | solution.py:254
  197.9 3.6 %fusion.18 = bf16[768,512]{1,0:T(8,128)(2,1)} fusion(bf16[1024,896]{0,1:T(8,128)(2,1)} %all-gather.4.cloned.1.call-done, bf16[1,1024,512]{2,1,0:T(8,128)(2,1)} %param.36), kind=kOutput, calls=%fused_computation.27 | convolution fusion | flops 805699584 | bytes 3407872 | tf_op jit(solution)/shard_map/fr,fd->rd/dot_general | solution.py:259
  201.4 4.6 %all-to-all-start.1 = ((bf16[8,96,512]{2,1,0:T(8,128)(2,1)}), bf16[8,96,512]{2,1,0:T(8,128)(2,1)S(1)}, u32[]{:S(2)}, u32[]{:S(2)}) async-start(bf16[8,96,512]{2,1,0:T(8,128)(2,1)} %bitcast.187), calls=%async_computation.2 | async-start | bytes 1572864 | tf_op jit(solution)/shard_map/all_to_all | solution.py:263
  206.5 20.5 %all-to-all-done.1 = bf16[8,96,512]{2,1,0:T(8,128)(2,1)S(1)} async-done(((bf16[8,96,512]{2,1,0:T(8,128)(2,1)}), bf16[8,96,512]{2,1,0:T(8,128)(2,1)S(1)}, u32[]{:S(2)}, u32[]{:S(2)}) %all-to-all-start.1) | async-done | bytes 786464 | tf_op jit(solution)/shard_map/all_to_all | solution.py:263
  227.0 2.0 gather_fusion.1
  230.0 2.3 fusion.37
  (167 shorter events, 36.6 us)
Async XLA Ops:
  8.0 170.2 %copy-start = (bf16[512,2048]{1,0:T(8,128)(2,1)S(1)}, bf16[512,2048]{1,0:T(8,128)(2,1)}, u32[]{:S(2)}) copy-start(bf16[512,2048]{1,0:T(8,128)(2,1)} %param.29) | copy-start | bytes 6291460
  16.7 0.8 copy-start.16
  21.8 29.6 %copy-start.24 = (bf16[256,512]{1,0:T(8,128)(2,1)S(1)}, bf16[256,512]{1,0:T(8,128)(2,1)}, u32[]{:S(2)}) copy-start(bf16[256,512]{1,0:T(8,128)(2,1)} %param.21) | copy-start | bytes 786436
  21.8 31.1 %copy-start.26 = (f32[512]{0:T(512)S(1)}, f32[512]{0:T(512)}, u32[]{:S(2)}) copy-start(f32[512]{0:T(512)} %param.26) | copy-start | bytes 6148
  24.1 27.3 %all-to-all-start = ((bf16[8,96,512]{2,1,0:T(8,128)(2,1)}), bf16[8,96,512]{2,1,0:T(8,128)(2,1)S(1)}, u32[]{:S(2)}, u32[]{:S(2)}) async-start(bf16[8,96,512]{2,1,0:T(8,128)(2,1)} %dynamic-slice_select_fusion), calls=%async_computation | async-start | bytes 1572864 | tf_op jit(solution)/shard_map/all_to_all | solution.py:222
  30.4 107.3 %all-gather.6.cloned.1.call-start = ((), (), s32[]{:S(2)}) async-start(), calls=%async_computation.5 | async-start | bytes 1179648 | tf_op jit(solution)/shard_map/all_gather | solution.py:144
  51.4 6.1 %copy-start.13 = (bf16[8,96,512]{2,1,0:T(8,128)(2,1)}, bf16[8,96,512]{2,1,0:T(8,128)(2,1)S(1)}, u32[]{:S(2)}) copy-start(bf16[8,96,512]{2,1,0:T(8,128)(2,1)S(1)} %all-to-all-done) | copy-start | bytes 2359300
  51.5 6.0 %copy-start.20 = (bf16[256,512]{0,1:T(8,128)(2,1)}, bf16[256,512]{0,1:T(8,128)(2,1)S(1)}, u32[]{:S(2)}) copy-start(bf16[256,512]{0,1:T(8,128)(2,1)S(1)} %copy.250) | copy-start | bytes 786436
  52.9 10.3 %copy-start.21 = (bf16[256,512]{0,1:T(8,128)(2,1)}, bf16[256,512]{0,1:T(8,128)(2,1)S(1)}, u32[]{:S(2)}) copy-start(bf16[256,512]{0,1:T(8,128)(2,1)S(1)} %copy.246) | copy-start | bytes 786436
  72.1 2.3 copy-start.7
  72.1 2.3 copy-start.11
  74.5 9.2 %copy-start.1 = (f32[4,8,128,128]{3,2,1,0:T(8,128)}, f32[4,8,128,128]{3,2,1,0:T(8,128)S(1)}, u32[]{:S(2)}) copy-start(f32[4,8,128,128]{3,2,1,0:T(8,128)S(1)} %fusion.5) | copy-start | bytes 6291460
  83.6 1.7 copy-start.22
  88.8 1.6 copy-start.5
  88.9 1.7 copy-start.15
  90.6 1.2 copy-start.12
  90.6 1.5 copy-start.19
  92.1 1.2 copy-start.6
  93.3 1.8 copy-start.9
  95.1 3.3 %copy-start.3 = (f32[4,8,64,128]{3,2,1,0:T(8,128)}, f32[4,8,64,128]{3,2,1,0:T(8,128)S(1)}, u32[]{:S(2)}) copy-start(f32[4,8,64,128]{3,2,1,0:T(8,128)S(1)} %convolution_subtract_fusion.5) | copy-start | bytes 3145732
  95.1 1.5 copy-start.14
  95.1 4.3 %copy-start.28 = (f32[512]{0:T(512)S(1)}, f32[512]{0:T(512)}, u32[]{:S(2)}) copy-start(f32[512]{0:T(512)} %param.28) | copy-start | bytes 6148
  95.1 4.4 %copy-start.17 = (bf16[128,2048]{1,0:T(8,128)(2,1)S(1)}, bf16[128,2048]{1,0:T(8,128)(2,1)}, u32[]{:S(2)}) copy-start(bf16[128,2048]{1,0:T(8,128)(2,1)} %copy-done.16) | copy-start | bytes 1572868
  96.6 20.0 %collective-permute-start = (bf16[768,512]{1,0:T(8,128)(2,1)S(1)}, bf16[768,512]{1,0:T(8,128)(2,1)}, u32[]{:S(2)}, u32[]{:S(2)}) collective-permute-start(bf16[768,512]{1,0:T(8,128)(2,1)S(1)} %bitcast.175), channel_id=1, source_target_pairs={{0,1},{1,2},{2,3},{3,0},{4,5},{5,6},{6,7},{7,4},{8,9},{9,10},{10,1... | collective-permute-start | bytes 2359304 | tf_op jit(solution)/shard_map/ppermute | solution.py:245
  99.3 98.5 %all-gather.4.cloned.1.call-start = ((), (), s32[]{:S(2)}) async-start(), calls=%async_computation.4 | async-start | bytes 2293760 | tf_op jit(solution)/shard_map/all_gather | solution.py:254
  99.5 20.5 %copy-start.2 = (f32[4,8,128,128]{3,2,1,0:T(8,128)S(1)}, f32[4,8,128,128]{3,2,1,0:T(8,128)}, u32[]{:S(2)}) copy-start(f32[4,8,128,128]{3,2,1,0:T(8,128)} %copy-done.1) | copy-start | bytes 6291460
  99.5 20.6 %copy-start.8 = (f32[4,8,64,64]{3,2,1,0:T(8,128)S(1)}, f32[4,8,64,64]{3,2,1,0:T(8,128)}, u32[]{:S(2)}) copy-start(f32[4,8,64,64]{3,2,1,0:T(8,128)} %copy-done.7) | copy-start | bytes 1572868
  99.5 20.6 %copy-start.10 = (f32[4,8,64,128]{3,2,1,0:T(8,128)S(1)}, f32[4,8,64,128]{3,2,1,0:T(8,128)}, u32[]{:S(2)}) copy-start(f32[4,8,64,128]{3,2,1,0:T(8,128)} %copy-done.9) | copy-start | bytes 3145732
  116.6 19.3 %collective-permute-start.1 = (bf16[768,512]{1,0:T(8,128)(2,1)}, bf16[768,512]{1,0:T(8,128)(2,1)}, u32[]{:S(2)}, u32[]{:S(2)}) collective-permute-start(bf16[768,512]{1,0:T(8,128)(2,1)} %collective-permute-done), channel_id=1, source_target_pairs={{0,1},{1,2},{2,3},{3,0},{4,5},{5,6},{6,7},{7,4},{8,9},{9,10},{10,1... | collective-permute-start | bytes 2359304 | tf_op jit(solution)/shard_map/ppermute | solution.py:245
  136.0 18.5 %collective-permute-start.2 = (bf16[768,512]{1,0:T(8,128)(2,1)}, bf16[768,512]{1,0:T(8,128)(2,1)}, u32[]{:S(2)}, u32[]{:S(2)}) collective-permute-start(bf16[768,512]{1,0:T(8,128)(2,1)} %collective-permute-done.1), channel_id=1, source_target_pairs={{0,1},{1,2},{2,3},{3,0},{4,5},{5,6},{6,7},{7,4},{8,9},{9,10},{10,1... | collective-permute-start | bytes 2359304 | tf_op jit(solution)/shard_map/ppermute | solution.py:245
  159.6 2.7 %copy-start.30 = (bf16[1,256,2048]{2,1,0:T(8,128)(2,1)S(1)}, bf16[1,256,2048]{2,1,0:T(8,128)(2,1)}, u32[]{:S(2)}) copy-start(bf16[1,256,2048]{2,1,0:T(8,128)(2,1)} %param.34) | copy-start | bytes 3145732
  162.3 1.2 copy-start.31
  164.6 6.1 %copy-start.4 = (f32[4,8,64,128]{3,2,1,0:T(8,128)S(1)}, f32[4,8,64,128]{3,2,1,0:T(8,128)}, u32[]{:S(2)}) copy-start(f32[4,8,64,128]{3,2,1,0:T(8,128)} %copy-done.3) | copy-start | bytes 3145732
  165.4 66.8 %reduce-scatter.2.cloned.1.call-start = ((), (), s32[]{:S(2)}) async-start(), calls=%async_computation.3 | async-start | bytes 1310720 | tf_op jit(solution)/shard_map/reduce_scatter | solution.py:173
  166.9 4.5 %copy-start.18 = (f32[4,8,64,128]{3,2,1,0:T(8,128)S(1)}, f32[4,8,64,128]{3,2,1,0:T(8,128)}, u32[]{:S(2)}) copy-start(f32[4,8,64,128]{3,2,1,0:T(8,128)} %convolution_subtract_fusion.6) | copy-start | bytes 3145732
  174.7 3.5 %copy-start.23 = (bf16[256,512]{1,0:T(8,128)(2,1)S(1)}, bf16[256,512]{1,0:T(8,128)(2,1)}, u32[]{:S(2)}) copy-start(bf16[256,512]{1,0:T(8,128)(2,1)} %param.22) | copy-start | bytes 786436
  174.7 3.5 %copy-start.27 = (f32[512]{0:T(512)S(1)}, f32[512]{0:T(512)}, u32[]{:S(2)}) copy-start(f32[512]{0:T(512)} %param.27) | copy-start | bytes 6148
  181.4 24.8 %copy-start.29 = (f32[128,4]{0,1:T(4,128)S(1)}, f32[128,4]{0,1:T(4,128)}, u32[]{:S(2)}) copy-start(f32[128,4]{0,1:T(4,128)} %param.32) | copy-start | bytes 6148
  181.4 24.9 %copy-start.25 = (s32[128,4]{0,1:T(4,128)S(1)}, s32[128,4]{0,1:T(4,128)}, u32[]{:S(2)}) copy-start(s32[128,4]{0,1:T(4,128)} %param.31) | copy-start | bytes 6148
  201.4 25.6 %all-to-all-start.1 = ((bf16[8,96,512]{2,1,0:T(8,128)(2,1)}), bf16[8,96,512]{2,1,0:T(8,128)(2,1)S(1)}, u32[]{:S(2)}, u32[]{:S(2)}) async-start(bf16[8,96,512]{2,1,0:T(8,128)(2,1)} %bitcast.187), calls=%async_computation.2 | async-start | bytes 1572864 | tf_op jit(solution)/shard_map/all_to_all | solution.py:263
Sparse Core Ops, SparseCore 0:
  99.5 19.8 all-gather.5
Sparse Core Ops, SparseCore 1:
  165.5 32.3 all-gather.3
  201.2 27.8 reduce-scatter.1
